TPU v7x, 32 devices: a whole 2x2x4 slice. The times are simulated.
32 devices in a mesh: ep: 8 (over z, y), tp: 4 (over x, core).
Axes of the slice: x: 2, y: 2, z: 4, core: 2. Of those that a mesh axis runs over, the one named last changes fastest.
Arguments:
- queries: bfloat16 [8192, 1024], P('ep', 'tp'), may hold values from -6 to 6
- keys: bfloat16 [8192, 1024], P('ep', 'tp'), may hold values from -6 to 6
- values: bfloat16 [8192, 2048], P('ep', 'tp'), may hold values from -6 to 6
- log_input_gate: float32 [8192, 8], P('ep', 'tp'), may hold values from -6 to 103
- forget_preactivation: float32 [8192, 8], P('ep', 'tp'), may hold values from 0 to 16
- forget_offset: float32 [8192, 8], P('ep', 'tp'), may hold values from -0.7 to 0
- head_norm_scale: float32 [2048], P('tp'), may hold values from 0.1 to 1.9
- memory_output_weight: bfloat16 [2048, 4096], P('tp'), may hold values from -0.125 to 0.125
- second_micro_tokens: bfloat16 [4096, 4096], P('ep'), may hold values from -6 to 6
- expert_norm_scale: float32 [4096], replicated, may hold values from 0.1 to 1.9
- expert_choice_index: int32 [4096, 2], P('ep'), may hold values from 0 to 15, all different within a row; in each aligned block of 512 rows (0 to 511, 512 to 1023, ...) at most 96 rows name the same one
- group_likelihood: float32 [4096], P('ep'), may hold values from 0.2 to 1
- expert_raw_weight: float32 [4096, 2], P('ep'), may hold values from 0.1 to 1
- gate_weight: bfloat16 [16, 4096, 1024], P('ep', None, 'tp'), may hold values from -0.09375 to 0.09375
- up_weight: bfloat16 [16, 4096, 1024], P('ep', None, 'tp'), may hold values from -0.09375 to 0.09375
- down_weight: bfloat16 [16, 1024, 4096], P('ep', 'tp'), may hold values from -0.1875 to 0.1875
Outputs:
- mixed: bfloat16 [8192, 4096], P(('ep', 'tp'))
- routed: bfloat16 [4096, 4096], P('ep', 'tp')
Inputs may be any that keep to these rules, and one draw needn't show every extreme that they name: `expert_choice_index`: each row names 2 different experts. Within the 512 rows of one index of ep (aligned blocks) no expert is named more than 96 times, and in some blocks one expert is named exactly 96 times.
All inputs are finite; a program needn't handle non-finite values.
Results may differ from a plain program's by a relative error of at most 0.012.
Values may be sent and summed in bfloat16 or wider, within the bound.
A program may use at most 192 MiB of HBM per device.

v0:
```python
import functools
import math

import jax
import jax.numpy as jnp
from jax import lax
from jax.experimental import pallas as pl
from jax.experimental.pallas import tpu as pltpu
from jax.sharding import PartitionSpec as P

BLOCK = 128
EPSILON = 1e-06
FLOOR_LOG = -1e30
LANES = 128
MESH = pl.DeviceIdType.MESH
F32 = jnp.float32
BF16 = jnp.bfloat16


def flip(index, mask):
    bit = 1
    while bit <= mask:
        if mask & bit:
            index = index + bit * (1 - 2 * ((index // bit) % 2))
        bit *= 2
    return index


def dot(left, right, dims=((1,), (0,))):
    return lax.dot_general(left, right, (dims, ((), ())), preferred_element_type=F32)


def kernel(
    n,
    tp,
    a_ref,
    b_ref,
    q_hbm,
    k_hbm,
    v_hbm,
    cols_ref,
    arow_ref,
    gp_ref,
    hscale_ref,
    wo_hbm,
    gate_hbm,
    up_hbm,
    down_hbm,
    mixed_ref,
    ret_ref,
    rows,
    gw,
    uw,
    dcols,
    fh,
    res,
    part,
    crecv,
    xrecv,
    qb,
    kb,
    vb,
    hid,
    wo,
    cst,
    cin,
    tabs,
    stat,
    stats,
    st_send,
    st_buf,
    low_send,
    low_buf,
    load_sem,
    a_send,
    a_recv,
    b_send,
    b_recv,
    f_send,
    f_recv,
    h_send,
    h_recv,
    w_send,
    w_recv,
    s_send,
    s_recv,
    t_send,
    t_recv,
    l_send,
    l_recv,
    m_send,
    m_recv,
    r_send,
    r_recv,
):
    me, t = lax.axis_index("ep"), lax.axis_index("tp")
    half = n // 2
    group_count = 4
    per_group = n // group_count
    local_experts, cap, width = a_ref.shape[1:]
    units = gw.shape[2]
    block_count, head_count = cst.shape[0] - 1, cst.shape[1]
    key_width, value_width = cst.shape[2:]
    row_count = qb.shape[0]
    part_rows = part.shape[1]
    model = rows.shape[2]
    t1, t2 = flip(t, 1), flip(t, 2)
    core, side = t % 2, t // 2
    base = (me // half) * half
    slot = me - base

    def peer(mask):
        return {"ep": flip(me, mask)}

    def window(index):
        return pl.ds(pl.multiple_of(index * width, LANES), width)

    def unit_window(index):
        return pl.ds(pl.multiple_of(index * units, LANES), units)

    def remote(src, dst, send, recv, device):
        return pltpu.make_async_remote_copy(
            src_ref=src,
            dst_ref=dst,
            send_sem=send,
            recv_sem=recv,
            device_id=device,
            device_id_type=MESH,
        )

    barrier = pltpu.get_barrier_semaphore()
    for mask in range(1, n):
        pl.semaphore_signal(barrier, inc=1, device_id=peer(mask), device_id_type=MESH)
    for mask in range(1, tp):
        pl.semaphore_signal(
            barrier, inc=1, device_id={"tp": flip(t, mask)}, device_id_type=MESH
        )

    loads = {}

    def load(name, src, dst):
        loads[name] = pltpu.make_async_copy(src, dst, load_sem.at[len(loads)])
        loads[name].start()

    load("k", k_hbm, kb)
    load("v", v_hbm, vb)
    load("q", q_hbm, qb)
    load("a0", a_ref.at[0], rows.at[:, pl.ds(0, cap), window(t)])
    load("b0", b_ref.at[0], rows.at[:, pl.ds(0, cap), window(t2)])
    load("wo", wo_hbm, wo)
    load("gate", gate_hbm, gw)
    load("up", up_hbm, uw)
    load("down", down_hbm.at[:, :, window(t)], dcols.at[:, unit_window(t), :])
    pl.semaphore_wait(barrier, n - 1 + tp - 1)

    sends = []

    def start(copy):
        copy.start()
        sends.append(copy)
        return copy

    def slots(mask, count=1):
        return pl.ds(mask * cap, count * cap)

    a_copy, b_copy = {}, {}

    def dispatch(mask):
        a_copy[mask] = start(
            remote(
                a_ref.at[mask],
                rows.at[:, slots(mask), window(t)],
                a_send.at[mask],
                a_recv.at[mask],
                peer(mask),
            )
        )
        if mask < half:
            b_copy[mask] = start(
                remote(
                    b_ref.at[mask],
                    rows.at[:, slots(mask), window(t2)],
                    b_send.at[mask],
                    b_recv.at[mask],
                    peer(mask),
                )
            )

    def forward_x(mask):
        a_copy[mask].wait_recv()
        view = rows.at[:, slots(mask), window(t)]
        b_copy[mask] = start(
            remote(view, view, b_send.at[mask], b_recv.at[mask], {"tp": t2})
        )

    group_masks = [range(g * per_group, (g + 1) * per_group) for g in range(group_count)]
    near_groups = [g for g in range(group_count) if group_masks[g][0] < half]
    dispatch(group_masks[2][0])
    w_copy = {}
    for mask in (2, 3, 1):
        w_copy[mask] = start(
            remote(
                down_hbm.at[:, :, window(flip(t, mask))],
                dcols.at[:, unit_window(t), :],
                w_send.at[mask],
                w_recv.at[mask],
                {"tp": flip(t, mask)},
            )
        )
    for mask in group_masks[0]:
        if mask:
            dispatch(mask)

    TQ, TC, TW1, TW2, TF, TWI, TWL = range(7)
    stable = jnp.full((1, LANES), FLOOR_LOG, F32)
    total = jnp.zeros((1, LANES), F32)
    for b in range(block_count):
        span, peak = gp_ref[0, b : b + 1, :], gp_ref[1, b : b + 1, :]
        tabs[TQ, b : b + 1, :] = total
        tabs[TC, b : b + 1, :] = stable
        newer = jnp.maximum(span + stable, peak)
        tabs[TW1, b : b + 1, :] = jnp.exp(span + stable - newer)
        tabs[TW2, b : b + 1, :] = jnp.exp(peak - newer)
        stable, total = newer, total + span
    stat[0:1, :] = stable
    stat[1:2, :] = total
    stats[me, 0:1, :] = stable
    stats[me, 1:2, :] = total

    loads["k"].wait()
    loads["v"].wait()
    cst[0] = jnp.zeros(cst.shape[1:], F32)

    def gather_block(b, carry):
        at = pl.ds(pl.multiple_of(b * BLOCK, BLOCK), BLOCK)
        for h in range(head_count):
            keyed = kb[at, h * key_width : (h + 1) * key_width].astype(F32)
            weight = cols_ref[at, head_count + h : head_count + h + 1]
            update = dot(
                (keyed * weight).astype(BF16),
                vb[at, h * value_width : (h + 1) * value_width],
                ((0,), (0,)),
            )
            old = tabs[TW1, pl.ds(b, 1), h : h + 1]
            new = tabs[TW2, pl.ds(b, 1), h : h + 1]
            cst[b + 1, h] = old * cst[b, h] + new * update
        return carry

    lax.fori_loop(0, block_count, gather_block, 0)
    st_send[...] = cst[block_count].astype(BF16)
    st_buf[slot] = cst[block_count].astype(BF16)
    s_copy = {
        mask: start(
            remote(stat, stats.at[me], s_send.at[mask], s_recv.at[mask], peer(mask))
        )
        for mask in range(1, n)
    }
    t_copy = {
        mask: start(
            remote(st_send, st_buf.at[slot], t_send.at[mask], t_recv.at[mask], peer(mask))
        )
        for mask in range(1, half)
    }
    for mask in group_masks[2][1:]:
        dispatch(mask)
    for mask in group_masks[1][: per_group // 2]:
        dispatch(mask)

    for mask in range(1, n):
        s_copy[mask].wait_recv()
    for mask in range(1, half):
        t_copy[mask].wait_recv()

    low_log, suffix = [None] * half, jnp.zeros((1, LANES), F32)
    for j in reversed(range(half)):
        low_log[j] = stats[j, 0:1, :] + suffix
        suffix = suffix + stats[j, 1:2, :]
    low_stable = functools.reduce(jnp.maximum, low_log)
    low_weight = [jnp.exp(value - low_stable) for value in low_log]

    l_copy = remote(
        low_send, low_buf, l_send.at[0], l_recv.at[0], {"ep": flip(me, half)}
    )

    @pl.when(me < half)
    def _():
        for h in range(head_count):
            summed = jnp.zeros((key_width, value_width), F32)
            for j in range(half):
                summed = summed + low_weight[j][:, h : h + 1] * st_buf[j, h].astype(F32)
            low_send[h] = summed.astype(BF16)
        low_buf[...] = jnp.zeros(low_buf.shape, BF16)
        l_copy.start()

    for mask in group_masks[3]:
        dispatch(mask)
    for mask in group_masks[1][per_group // 2 :]:
        dispatch(mask)

    for mask in group_masks[2]:
        forward_x(mask)

    logs, valid, suffix = [None] * half, [None] * half, jnp.zeros((1, LANES), F32)
    for j in reversed(range(half)):
        valid[j] = j < slot
        logs[j] = jnp.where(valid[j], stats[base + j, 0:1, :] + suffix, FLOOR_LOG)
        suffix = jnp.where(valid[j], suffix + stats[base + j, 1:2, :], suffix)
    low_in = jnp.where(me >= half, low_stable + suffix, FLOOR_LOG)
    peak_in = functools.reduce(jnp.maximum, logs + [low_in])
    weights = [
        jnp.where(valid[j], jnp.exp(logs[j] - peak_in), 0.0) for j in range(half)
    ]
    low_in = jnp.where(me >= half, jnp.exp(low_in - peak_in), 0.0)
    carried_stable = tabs[TQ] + peak_in
    full_stable = jnp.maximum(carried_stable, tabs[TC])
    tabs[TF] = full_stable
    tabs[TWI] = jnp.exp(carried_stable - full_stable)
    tabs[TWL] = jnp.exp(tabs[TC] - full_stable)

    @pl.when(me >= half)
    def _():
        l_copy.wait_recv()

    for h in range(head_count):
        summed = low_in[:, h : h + 1] * low_buf[h].astype(F32)
        for j in range(half):
            summed = summed + weights[j][:, h : h + 1] * st_buf[j, h].astype(F32)
        cin[h] = summed

    loads["q"].wait()
    scale = 1.0 / math.sqrt(key_width)
    causal = lax.broadcasted_iota(jnp.int32, (BLOCK, BLOCK), 0) >= lax.broadcasted_iota(
        jnp.int32, (BLOCK, BLOCK), 1
    )

    def read_block(b, carry):
        at = pl.ds(pl.multiple_of(b * BLOCK, BLOCK), BLOCK)
        for h in range(head_count):
            query = qb[at, h * key_width : (h + 1) * key_width]
            key = kb[at, h * key_width : (h + 1) * key_width]
            value = vb[at, h * value_width : (h + 1) * value_width]
            running = cols_ref[at, h : h + 1]
            other = arow_ref[pl.ds(h * block_count + b, 1), :]
            scores = dot(query, key, ((1,), (1,))) * scale
            log_weight = jnp.where(causal, running + other, FLOOR_LOG)
            carried = running + tabs[TF, pl.ds(b, 1), h : h + 1]
            highest = jnp.maximum(carried, jnp.max(log_weight, axis=1, keepdims=True))
            inner = (scores * jnp.exp(log_weight - highest)).astype(BF16)
            memory = (
                tabs[TWI, pl.ds(b, 1), h : h + 1] * cin[h]
                + tabs[TWL, pl.ds(b, 1), h : h + 1] * cst[b, h]
            ).astype(BF16)
            state = jnp.exp(carried - highest) * dot(query, memory) + dot(inner, value)
            mean = jnp.mean(state * state, axis=1, keepdims=True)
            state = state * lax.rsqrt(mean + EPSILON)
            at_head = slice(h * value_width, (h + 1) * value_width)
            hid[at, at_head] = (state * hscale_ref[:, at_head]).astype(BF16)
        return carry

    lax.fori_loop(0, block_count, read_block, 0)

    loads["wo"].wait()
    tile = 256

    def project(index):
        left = hid[pl.ds(pl.multiple_of(index * part_rows, part_rows), part_rows), :]

        def piece(i, carry):
            at = pl.ds(pl.multiple_of(i * tile, tile), tile)
            part[index, :, at] = dot(left, wo[:, at]).astype(BF16)
            return carry

        lax.fori_loop(0, model // tile, piece, 0)

    m_copy = []
    for i in range(2):
        project(2 * i + 1 - core)
        m_copy.append(
            start(
                remote(
                    part.at[2 * i + 1 - core],
                    crecv.at[i],
                    m_send.at[i],
                    m_recv.at[i],
                    {"tp": t1},
                )
            )
        )
    project(t2)
    for copy in m_copy:
        copy.wait_recv()
    chunk = 32

    def add_other(i, carry):
        at = pl.ds(pl.multiple_of(i * chunk, chunk), chunk)
        part[t2, at, :] = (
            part[t2, at, :].astype(F32) + crecv[1 - side, at, :].astype(F32)
        ).astype(BF16)
        return carry

    lax.fori_loop(0, part_rows // chunk, add_other, 0)

    f_copy, h_copy = {}, {}

    def stage_core(g, which):
        if which == 0:
            for mask in group_masks[g]:
                if mask == 0:
                    loads["a0"].wait()
                elif mask < half:
                    a_copy[mask].wait_recv()
        else:
            for mask in group_masks[g]:
                if mask == 0:
                    loads["b0"].wait()
                else:
                    b_copy[mask].wait_recv()
        view = rows.at[
            :, slots(group_masks[g][0], per_group), window(t if which == 0 else t2)
        ]
        f_copy[g, which] = start(
            remote(view, view, f_send.at[which, g], f_recv.at[which, g], {"tp": t1})
        )

    def group_slots(g):
        return slots(group_masks[g][0], per_group)

    def send_units(g, kind, owner, target):
        view = fh.at[:, group_slots(g), unit_window(owner)]
        h_copy[g, kind] = start(
            remote(view, view, h_send.at[kind, g], h_recv.at[kind, g], {"tp": target})
        )

    weights_ready = []

    def stage_hidden(g):
        f_copy[g, 0].wait_recv()
        f_copy[g, 1].wait_recv()
        if not weights_ready:
            loads["gate"].wait()
            loads["up"].wait()
            weights_ready.append(True)

        def one(e, carry):
            left = rows[e, group_slots(g), :]
            gate = dot(left, gw[e])
            upward = dot(left, uw[e])
            fh[e, group_slots(g), unit_window(t)] = (
                gate * jax.nn.sigmoid(gate) * upward
            ).astype(BF16)
            return carry

        lax.fori_loop(0, local_experts, one, 0)
        send_units(g, 0, t, t2)
        send_units(g, 1, t, t1)

    def stage_units(g):
        h_copy[g, 0].wait_recv()
        send_units(g, 2, t2, t1)

    down_ready = []
    r_copy = {}

    def stage_down(g):
        h_copy[g, 1].wait_recv()
        h_copy[g, 2].wait_recv()
        if not down_ready:
            loads["down"].wait()
            for mask in (1, 2, 3):
                w_copy[mask].wait_recv()
            down_ready.append(True)

        def one(i, carry):
            e, c = i // (width // tile), i % (width // tile)
            at = pl.ds(pl.multiple_of(c * tile, tile), tile)
            res[e, group_slots(g), at] = dot(
                fh[e, group_slots(g), :], dcols[e, :, at]
            ).astype(BF16)
            return carry

        lax.fori_loop(0, local_experts * (width // tile), one, 0)
        for mask in group_masks[g]:
            view = res.at[:, slots(mask), :]
            if mask:
                r_copy[mask] = start(
                    remote(
                        view, ret_ref.at[mask], r_send.at[mask], r_recv.at[mask], peer(mask)
                    )
                )
            else:
                load("ret", view, ret_ref.at[0])

    stage_core(2, 0)
    stage_core(2, 1)
    x_copy = start(
        remote(part.at[t2], xrecv, m_send.at[2], m_recv.at[2], {"tp": t2})
    )
    stage_core(0, 0)
    stage_core(0, 1)
    project(t)
    stage_hidden(2)
    stage_hidden(0)
    stage_units(2)
    for mask in group_masks[3]:
        forward_x(mask)
    stage_core(3, 0)
    stage_units(0)
    stage_down(2)
    stage_core(3, 1)
    stage_core(1, 0)
    stage_core(1, 1)
    stage_down(0)
    stage_hidden(3)
    stage_hidden(1)
    stage_units(3)
    stage_units(1)
    stage_down(3)
    stage_down(1)

    x_copy.wait_recv()

    def add_own(i, carry):
        at = pl.ds(pl.multiple_of(i * chunk, chunk), chunk)
        mixed_ref[at, :] = (
            part[t, at, :].astype(F32)
            + crecv[side, at, :].astype(F32)
            + xrecv[at, :].astype(F32)
        ).astype(BF16)
        return carry

    lax.fori_loop(0, part_rows // chunk, add_own, 0)

    loads["ret"].wait()
    for mask in range(1, n):
        r_copy[mask].wait_recv()
    for copy in sends:
        copy.wait_send()

    @pl.when(me < half)
    def _():
        l_copy.wait_send()


def gates(log_input_gate, forget_preactivation, forget_offset, key_width):
    row_count, head_count = log_input_gate.shape
    block_count = row_count // BLOCK
    forget_log = jax.nn.log_sigmoid(forget_preactivation) + forget_offset
    forget_log = forget_log.reshape(block_count, BLOCK, head_count)
    in_gate = log_input_gate.reshape(block_count, BLOCK, head_count)
    lower = jnp.tril(jnp.ones((BLOCK, BLOCK), F32))
    running = jnp.einsum(
        "ts,bsh->bth",
        lower,
        forget_log,
        preferred_element_type=F32,
        precision=lax.Precision.HIGHEST,
    )
    totals = running[:, -1]
    to_end = totals[:, None] - running + in_gate
    peak = jnp.max(to_end, axis=1)
    key_weight = jnp.exp(to_end - peak[:, None]) * (1.0 / math.sqrt(key_width))
    cols = jnp.concatenate([running, key_weight], axis=2).reshape(row_count, -1)
    arow = (in_gate - running).transpose(2, 0, 1).reshape(head_count * block_count, BLOCK)
    gp = jnp.pad(jnp.stack([totals, peak]), ((0, 0), (0, 0), (0, LANES - head_count)))
    return cols, arow, gp


def per_device(
    queries,
    keys,
    values,
    log_input_gate,
    forget_preactivation,
    forget_offset,
    head_norm_scale,
    memory_output_weight,
    second_micro_tokens,
    expert_norm_scale,
    expert_choice_index,
    group_likelihood,
    expert_raw_weight,
    gate_weight,
    up_weight,
    down_weight,
):
    token_count, model_width = second_micro_tokens.shape
    pick_count = expert_choice_index.shape[1]
    local_experts, _, units = gate_weight.shape
    n, tp = lax.axis_size("ep"), lax.axis_size("tp")
    me, t = lax.axis_index("ep"), lax.axis_index("tp")
    half = n // 2
    expert_count = local_experts * n
    cap = tp * max(1, 3 * pick_count * token_count // (2 * expert_count * tp))
    width = model_width // tp
    row_count, head_count = log_input_gate.shape
    key_width = queries.shape[1] // head_count
    value_width = values.shape[1] // head_count
    block_count = row_count // BLOCK
    out_depth = head_count * value_width

    share = expert_raw_weight / jnp.sum(expert_raw_weight, axis=1, keepdims=True)
    route_weight = group_likelihood[:, None] * share

    experts = jnp.arange(expert_count, dtype=jnp.int32)
    named = expert_choice_index[:, :, None] == experts
    named_token = jnp.sum(named.astype(F32), axis=1)
    earlier = jnp.tril(jnp.ones((token_count, token_count), BF16), -1)
    before = jnp.dot(earlier, named_token.astype(BF16), preferred_element_type=F32)
    slot_rank = jnp.sum(jnp.where(named, before[:, None, :], 0.0), axis=2).astype(jnp.int32)
    slot_index = expert_choice_index * cap + slot_rank

    send_shape = (n, local_experts, cap)
    step, expert, row = (lax.broadcasted_iota(jnp.int32, send_shape, i) for i in range(3))
    send_slot = (((me ^ step) * local_experts + expert) * cap + row).reshape(-1)

    token_float = second_micro_tokens.astype(F32)
    inverse = lax.rsqrt(jnp.mean(token_float * token_float, axis=-1, keepdims=True) + EPSILON)

    def normed(index):
        tokens = lax.dynamic_slice_in_dim(second_micro_tokens, index * width, width, 1)
        gain = lax.dynamic_slice_in_dim(expert_norm_scale, index * width, width, 0)
        return (tokens.astype(F32) * inverse * gain).astype(BF16)

    chosen = send_slot[:, None] == slot_index[:, 0][None, :]
    for pick in range(1, pick_count):
        chosen = chosen | (send_slot[:, None] == slot_index[:, pick][None, :])
    chosen = chosen.astype(BF16)
    near = half * local_experts * cap
    out_a = jnp.dot(chosen, normed(t), preferred_element_type=F32).astype(BF16)
    out_b = jnp.dot(chosen[:near], normed(t ^ 2), preferred_element_type=F32).astype(BF16)
    out_a = out_a.reshape(n, local_experts, cap, width)
    out_b = out_b.reshape(half, local_experts, cap, width)

    cols, arow, gp = gates(log_input_gate, forget_preactivation, forget_offset, key_width)

    slot_rows = n * cap
    part_rows = row_count // tp
    vmem = pl.BlockSpec(memory_space=pltpu.VMEM)
    hbm = pl.BlockSpec(memory_space=pl.ANY)
    dma = pltpu.SemaphoreType.DMA
    mixed, returned = pl.pallas_call(
        functools.partial(kernel, n, tp),
        out_shape=(
            jax.ShapeDtypeStruct((part_rows, model_width), BF16),
            jax.ShapeDtypeStruct((n, local_experts, cap, width), BF16),
        ),
        in_specs=[hbm] * 5 + [vmem] * 4 + [hbm] * 4,
        out_specs=(vmem, hbm),
        scratch_shapes=[
            pltpu.VMEM((local_experts, slot_rows, model_width), BF16),
            pltpu.VMEM(gate_weight.shape, BF16),
            pltpu.VMEM(up_weight.shape, BF16),
            pltpu.VMEM((local_experts, tp * units, width), BF16),
            pltpu.VMEM((local_experts, slot_rows, tp * units), BF16),
            pltpu.VMEM((local_experts, slot_rows, width), BF16),
            pltpu.VMEM((tp, part_rows, model_width), BF16),
            pltpu.VMEM((2, part_rows, model_width), BF16),
            pltpu.VMEM((part_rows, model_width), BF16),
            pltpu.VMEM(queries.shape, BF16),
            pltpu.VMEM(keys.shape, BF16),
            pltpu.VMEM(values.shape, BF16),
            pltpu.VMEM((row_count, out_depth), BF16),
            pltpu.VMEM((out_depth, model_width), BF16),
            pltpu.VMEM((block_count + 1, head_count, key_width, value_width), F32),
            pltpu.VMEM((head_count, key_width, value_width), F32),
            pltpu.VMEM((7, block_count, LANES), F32),
            pltpu.VMEM((8, LANES), F32),
            pltpu.VMEM((n, 8, LANES), F32),
            pltpu.VMEM((head_count, key_width, value_width), BF16),
            pltpu.VMEM((half, head_count, key_width, value_width), BF16),
            pltpu.VMEM((head_count, key_width, value_width), BF16),
            pltpu.VMEM((head_count, key_width, value_width), BF16),
            dma((10,)),
            dma((n,)),
            dma((n,)),
            dma((n,)),
            dma((n,)),
            dma((2, 4)),
            dma((2, 4)),
            dma((3, 4)),
            dma((3, 4)),
            dma((tp,)),
            dma((tp,)),
            dma((n,)),
            dma((n,)),
            dma((half,)),
            dma((half,)),
            dma((1,)),
            dma((1,)),
            dma((3,)),
            dma((3,)),
            dma((n,)),
            dma((n,)),
        ],
        compiler_params=pltpu.CompilerParams(
            collective_id=0, has_side_effects=True, vmem_limit_bytes=67043328
        ),
        name="exchange",
    )(
        out_a,
        out_b,
        queries,
        keys,
        values,
        cols,
        arow,
        gp,
        head_norm_scale.reshape(1, -1),
        memory_output_weight,
        gate_weight,
        up_weight,
        down_weight,
    )
    returned = returned.reshape(-1, width)

    spread = jnp.zeros((token_count, send_slot.shape[0]), F32)
    for pick in range(pick_count):
        spread = spread + jnp.where(
            slot_index[:, pick : pick + 1] == send_slot[None, :],
            route_weight[:, pick : pick + 1],
            0.0,
        )
    spread_high = spread.astype(BF16)
    spread_low = (spread - spread_high.astype(F32)).astype(BF16)
    combined = jnp.dot(spread_high, returned, preferred_element_type=F32) + jnp.dot(
        spread_low, returned, preferred_element_type=F32
    )
    return mixed, combined.astype(BF16)


def solution(mesh):
    in_specs = (
        P("ep", "tp"),
        P("ep", "tp"),
        P("ep", "tp"),
        P("ep", "tp"),
        P("ep", "tp"),
        P("ep", "tp"),
        P("tp"),
        P("tp", None),
        P("ep", None),
        P(),
        P("ep", None),
        P("ep"),
        P("ep", None),
        P("ep", None, "tp"),
        P("ep", None, "tp"),
        P("ep", "tp", None),
    )
    out_specs = (P(("ep", "tp"), None), P("ep", "tp"))
    return jax.shard_map(
        per_device, mesh=mesh, in_specs=in_specs, out_specs=out_specs, check_vma=False
    )
```

profile of v0, /device:TPU:0, one launch (start us, length us, event | category | flops | bytes accessed | tf_op | source)
XLA Modules:
  0.0 228.5 jit_solution(676896434084802668)
XLA Ops:
  0.6 0.7 fusion.43
  1.4 0.7 convert_reduce_fusion
  2.1 0.3 fusion.18
  2.4 0.7 select_reduce_fusion
  3.1 0.7 convert_add_fusion
  3.9 0.1 add.78
  4.0 3.2 %multiply_reduce_fusion = f32[512]{0:T(512)S(1)} fusion(bf16[512,4096]{1,0:T(8,128)(2,1)} %param.24), kind=kLoop, calls=%fused_computation | loop fusion | flops 6290944 | bytes 4196352 | tf_op jit(solution)/shard_map/reduce_sum | solution.py:617
  7.3 0.2 copy-done
  7.5 3.6 %convolution_convert_fusion = bf16[1536,1024]{1,0:T(8,128)(2,1)} fusion(f32[1024]{0:T(1024)S(1)} %get-tuple-element.9, f32[512]{0:T(512)S(1)} %add_rsqrt_fusion, bf16[512,4096]{1,0:T(8,128)(2,1)S(1)} %copy-done, s32[]{:T(128)S(6)} %select_n.34, s32[512]{0:T(512)S(1)} %bitcast.53, s32[512]{0:T(512)S(1)} %bitcast.49, s32[1536]{0:T(1024)S(1)} %add.78), kind=kOutput, calls=%fused_computation.1 | convolution fusion | flops 1616642048 | bytes 4212740 | tf_op jit(solution)/shard_map/dot_general | solution.py:629
  11.1 0.9 compare_or_fusion
  12.0 2.3 %convolution_convert_fusion.1 = bf16[768,1024]{1,0:T(8,128)(2,1)} fusion(pred[1536,512]{1,0:T(32,128)(4,1)S(1)} %compare_or_fusion, f32[1024]{0:T(1024)S(1)} %get-tuple-element.8, bf16[512,4096]{1,0:T(8,128)(2,1)S(1)} %copy-done, s32[]{:T(128)S(6)} %select_n.35, f32[512]{0:T(512)S(1)} %add_rsqrt_fusion), kind=kOutput, calls=%fused_computation.9 | convolution fusion | flops 808189952 | bytes 3020804 | tf_op jit(solution)/shard_map/dot_general | solution.py:630
  14.4 0.2 convolution_bitcast_fusion
  14.5 0.2 slice_reduce_fusion
  14.8 0.2 fusion.34
  14.9 0.6 fusion.31
  15.5 1.0 copy.32
  16.6 0.1 copy.33
  16.6 0.6 pad.4.gp_ref
  17.3 201.2 %exchange.1 = (bf16[256,4096]{1,0:T(8,128)(2,1)}, bf16[8,2,96,1024]{3,2,1,0:T(8,128)(2,1)}) custom-call(bf16[8,2,96,1024]{3,2,1,0:T(8,128)(2,1)} %bitcast.42, bf16[4,2,96,1024]{3,2,1,0:T(8,128)(2,1)} %bitcast.44, bf16[1024,256]{1,0:T(8,128)(2,1)} %q_hbm.1, bf16[1024,256]{1,0:T(8,128)(2,1)} %k_hbm.1, bf16[1024,512]{1,0:T(8,128)(2,1)} %v_hbm.1, ...), custom_call_target="tpu_custom_call" | custom-call | tf_op jit(solution)/shard_map/exchange/pallas_call | solution.py:641
  218.5 0.7 reduce_sum.39
  219.2 0.7 divide_multiply_fusion
  219.9 4.0 %fusion.1 = f32[512,1024]{1,0:T(8,128)S(1)} fusion(bf16[1536,1024]{1,0:T(8,128)(2,1)} %bitcast.62, f32[512]{0:T(512)S(1)} %bitcast.59, f32[512]{0:T(512)S(1)} %bitcast.57, s32[1536]{0:T(1024)} %copy-done.2, s32[512]{0:T(512)} %bitcast.55, s32[512]{0:T(512)} %bitcast.51), kind=kOutput, calls=%fused_computation.10 | convolution fusion | flops 1617690624 | bytes 5257216 | tf_op jit(solution)/shard_map/dot_general | solution.py:725
  224.0 3.2 %add_convert_fusion = bf16[512,1024]{1,0:T(8,128)(2,1)} fusion(f32[512,1024]{1,0:T(8,128)S(1)} %fusion.1, bf16[1536,1024]{1,0:T(8,128)(2,1)S(1)} %bitcast.63, f32[512]{0:T(512)S(1)} %bitcast.60, f32[512]{0:T(512)S(1)} %bitcast.58, s32[1536]{0:T(1024)S(1)} %copy-done.3, s32[512]{0:T(512)S(1)} %bitcast.56, s32[512]{0:T(512)S(1)} %bitcast.52), kind=kOutput, calls=%fused_computation.6 | convolution fusion | flops 1616379904 | bytes 6305792 | tf_op jit(solution)/shard_map/dot_general | solution.py:725
  227.2 1.3 copy.48
  (32 shorter events, 0.2 us)
Async XLA Ops:
  3.8 7.3 %copy-start.5 = (s32[512,1]{0,1:T(1,128)}, s32[512,1]{0,1:T(1,128)S(1)}, u32[]{:S(2)}) copy-start(s32[512,1]{0,1:T(1,128)S(1)} %get-tuple-element.12) | copy-start | bytes 6148
  3.8 7.3 %copy-start.7 = (s32[512,1]{0,1:T(1,128)}, s32[512,1]{0,1:T(1,128)S(1)}, u32[]{:S(2)}) copy-start(s32[512,1]{0,1:T(1,128)S(1)} %get-tuple-element.13) | copy-start | bytes 6148
  4.0 7.1 %copy-start.2 = (s32[1536]{0:T(1024)}, s32[1536]{0:T(1024)S(1)}, u32[]{:S(2)}) copy-start(s32[1536]{0:T(1024)S(1)} %add.78) | copy-start | bytes 18436
  4.0 3.5 %copy-start = (bf16[512,4096]{1,0:T(8,128)(2,1)S(1)}, bf16[512,4096]{1,0:T(8,128)(2,1)}, u32[]{:S(2)}) copy-start(bf16[512,4096]{1,0:T(8,128)(2,1)} %param.24) | copy-start | bytes 12582916
  12.0 2.3 %copy-start.9 = (f32[1024,2]{0,1:T(2,128)S(1)}, f32[1024,2]{0,1:T(2,128)}, u32[]{:S(2)}) copy-start(f32[1024,2]{0,1:T(2,128)} %param.21) | copy-start | bytes 24580
  12.0 2.3 %copy-start.10 = (f32[1024,2]{0,1:T(2,128)S(1)}, f32[1024,2]{0,1:T(2,128)}, u32[]{:S(2)}) copy-start(f32[1024,2]{0,1:T(2,128)} %param.20) | copy-start | bytes 24580
  12.0 2.7 %copy-start.4 = (f32[1024,2]{0,1:T(2,128)S(1)}, f32[1024,2]{0,1:T(2,128)}, u32[]{:S(2)}) copy-start(f32[1024,2]{0,1:T(2,128)} %param.19) | copy-start | bytes 24580
  219.9 4.1 %copy-start.3 = (s32[1536]{0:T(1024)S(1)}, s32[1536]{0:T(1024)}, u32[]{:S(2)}) copy-start(s32[1536]{0:T(1024)} %copy-done.2) | copy-start | bytes 18436
  219.9 4.1 %copy-start.6 = (s32[512,1]{0,1:T(1,128)S(1)}, s32[512,1]{0,1:T(1,128)}, u32[]{:S(2)}) copy-start(s32[512,1]{0,1:T(1,128)} %copy-done.5) | copy-start | bytes 6148
  219.9 4.1 %copy-start.8 = (s32[512,1]{0,1:T(1,128)S(1)}, s32[512,1]{0,1:T(1,128)}, u32[]{:S(2)}) copy-start(s32[512,1]{0,1:T(1,128)} %copy-done.7) | copy-start | bytes 6148
  219.9 4.1 %copy-start.11 = (bf16[8,2,96,1024]{3,2,1,0:T(8,128)(2,1)S(1)}, bf16[8,2,96,1024]{3,2,1,0:T(8,128)(2,1)}, u32[]{:S(2)}) copy-start(bf16[8,2,96,1024]{3,2,1,0:T(8,128)(2,1)} %get-tuple-element.5) | copy-start | bytes 9437188
  224.0 3.2 %copy-start.1 = (bf16[256,4096]{1,0:T(8,128)(2,1)S(1)}, bf16[256,4096]{1,0:T(8,128)(2,1)}, u32[]{:S(2)}) copy-start(bf16[256,4096]{1,0:T(8,128)(2,1)} %get-tuple-element.16) | copy-start | bytes 6291460
where the time goes:
time: 231 us; the launch traced here: 229 us
  Pallas kernels  201 us (87%)
  matrix products  13.6 us (6%)
  other arithmetic  8.56 us (4%)
  local copies, waits for them, and re-layouts  4.31 us (2%)
    pallas_call x1, Pallas kernels, per_device(): pl.pallas_call(functools.partial(kernel, n, tp), out_shape=(jax.ShapeDtyp...  201 us

commit v1 on v0

--- a/solution.py
+++ b/solution.py
@@ -33,8 +33,12 @@
 def kernel(
     n,
     tp,
-    a_ref,
-    b_ref,
+    cap,
+    tok_hbm,
+    gain_ref,
+    choice_ref,
+    likelihood_ref,
+    raw_ref,
     q_hbm,
     k_hbm,
     v_hbm,
@@ -46,8 +50,8 @@
     gate_hbm,
     up_hbm,
     down_hbm,
-    mixed_ref,
-    ret_ref,
+    xrecv,
+    routed_ref,
     rows,
     gw,
     uw,
@@ -56,21 +60,23 @@
     res,
     part,
     crecv,
-    xrecv,
     qb,
     kb,
     vb,
     hid,
     wo,
     cst,
-    cin,
     tabs,
     stat,
     stats,
-    st_send,
     st_buf,
     low_send,
     low_buf,
+    ret,
+    other_nb,
+    bbuf,
+    route_col,
+    slot_row,
     load_sem,
     a_send,
     a_recv,
@@ -97,7 +103,10 @@
     half = n // 2
     group_count = 4
     per_group = n // group_count
-    local_experts, cap, width = a_ref.shape[1:]
+    local_experts, _, width = res.shape
+    token_count = routed_ref.shape[0]
+    nb = (routed_ref, other_nb)
+    rows_sent = local_experts * cap
     units = gw.shape[2]
     block_count, head_count = cst.shape[0] - 1, cst.shape[1]
     key_width, value_width = cst.shape[2:]
@@ -142,18 +151,19 @@
         loads[name] = pltpu.make_async_copy(src, dst, load_sem.at[len(loads)])
         loads[name].start()
 
+    token_tiles = token_count // part_rows
+    load("tokens", tok_hbm, part.at[pl.ds(0, token_tiles)])
     load("k", k_hbm, kb)
     load("v", v_hbm, vb)
     load("q", q_hbm, qb)
-    load("a0", a_ref.at[0], rows.at[:, pl.ds(0, cap), window(t)])
-    load("b0", b_ref.at[0], rows.at[:, pl.ds(0, cap), window(t2)])
     load("wo", wo_hbm, wo)
     load("gate", gate_hbm, gw)
     load("up", up_hbm, uw)
     load("down", down_hbm.at[:, :, window(t)], dcols.at[:, unit_window(t), :])
     pl.semaphore_wait(barrier, n - 1 + tp - 1)
 
-    sends = []
+    sends, sent = [], set()
+    tile, wide = 256, 512
 
     def start(copy):
         copy.start()
@@ -165,10 +175,33 @@
 
     a_copy, b_copy = {}, {}
 
+    def select(mask, which, store):
+        first = flip(me, mask) * rows_sent
+        ids = lax.broadcasted_iota(jnp.int32, (rows_sent, token_count), 0) + first
+        ids = ids.astype(F32)
+        chosen = (slot_row[4:5, :] == ids) | (slot_row[5:6, :] == ids)
+        chosen = jnp.where(chosen, 1.0, 0.0).astype(BF16)
+
+        def piece(i, carry):
+            at = pl.multiple_of(i * wide, wide)
+            picked = dot(chosen, nb[which][:, pl.ds(at, wide)])
+            for e in range(local_experts):
+                store(e, at, picked[e * cap : (e + 1) * cap].astype(BF16))
+            return carry
+
+        lax.fori_loop(0, width // wide, piece, 0)
+
     def dispatch(mask):
+        def store_a(e, at, value):
+            res[e, slots(mask), pl.ds(at, wide)] = value
+
+        def store_b(e, at, value):
+            bbuf[mask - 1, e, :, pl.ds(at, wide)] = value
+
+        select(mask, 0, store_a)
         a_copy[mask] = start(
             remote(
-                a_ref.at[mask],
+                res.at[:, slots(mask), :],
                 rows.at[:, slots(mask), window(t)],
                 a_send.at[mask],
                 a_recv.at[mask],
@@ -176,9 +209,10 @@
             )
         )
         if mask < half:
+            select(mask, 1, store_b)
             b_copy[mask] = start(
                 remote(
-                    b_ref.at[mask],
+                    bbuf.at[mask - 1],
                     rows.at[:, slots(mask), window(t2)],
                     b_send.at[mask],
                     b_recv.at[mask],
@@ -186,6 +220,15 @@
                 )
             )
 
+    def keep_own():
+        for which, owner in enumerate((t, t2)):
+
+            def store(e, at, value):
+                begin = pl.multiple_of(owner * width + at, wide)
+                rows[e, slots(0), pl.ds(begin, wide)] = value
+
+            select(0, which, store)
+
     def forward_x(mask):
         a_copy[mask].wait_recv()
         view = rows.at[:, slots(mask), window(t)]
@@ -194,19 +237,60 @@
         )
 
     group_masks = [range(g * per_group, (g + 1) * per_group) for g in range(group_count)]
-    near_groups = [g for g in range(group_count) if group_masks[g][0] < half]
-    dispatch(group_masks[2][0])
     w_copy = {}
-    for mask in (2, 3, 1):
-        w_copy[mask] = start(
+
+    def send_down(mask, e):
+        w_copy[mask, e] = start(
             remote(
-                down_hbm.at[:, :, window(flip(t, mask))],
-                dcols.at[:, unit_window(t), :],
-                w_send.at[mask],
-                w_recv.at[mask],
+                down_hbm.at[e, :, window(flip(t, mask))],
+                dcols.at[e, unit_window(t), :],
+                w_send.at[mask, e],
+                w_recv.at[mask, e],
                 {"tp": flip(t, mask)},
             )
         )
+
+    for mask in (2, 1):
+        for e in range(local_experts):
+            send_down(mask, e)
+    loads["tokens"].wait()
+    strip = 32
+
+    def normalize(i, carry):
+        which, first = i // (part_rows // strip), i % (part_rows // strip)
+        at = pl.ds(pl.multiple_of(first * strip, strip), strip)
+        to = pl.ds(pl.multiple_of(i * strip, strip), strip)
+        full = part[which, at, :].astype(F32)
+        mean = jnp.mean(full * full, axis=1, keepdims=True)
+        inverse = lax.rsqrt(mean + EPSILON)
+        for k, owner in enumerate((t, t2)):
+            piece = part[which, at, window(owner)].astype(F32)
+            nb[k][to, :] = (piece * inverse * gain_ref[:, window(owner)]).astype(BF16)
+        return carry
+
+    lax.fori_loop(0, token_count // strip, normalize, 0)
+    line = lax.broadcasted_iota(jnp.int32, (LANES, token_count), 0)
+    raw_sum = raw_ref[0:1, :] + raw_ref[1:2, :]
+    packed = jnp.zeros((LANES, token_count), F32)
+    for j in range(2):
+        share = likelihood_ref[...] * (raw_ref[j : j + 1, :] / raw_sum)
+        packed = jnp.where(line == j, choice_ref[j : j + 1, :].astype(F32), packed)
+        packed = jnp.where(line == 2 + j, share, packed)
+    placed = jnp.transpose(packed)
+    lane = lax.broadcasted_iota(jnp.int32, (token_count, LANES), 1).astype(F32)
+    named = [placed[:, j : j + 1] == lane for j in range(2)]
+    counted = sum(jnp.where(mask, 1.0, 0.0) for mask in named).astype(BF16)
+    earlier = lax.broadcasted_iota(
+        jnp.int32, (token_count, token_count), 0
+    ) > lax.broadcasted_iota(jnp.int32, (token_count, token_count), 1)
+    before = dot(jnp.where(earlier, 1.0, 0.0).astype(BF16), counted)
+    for j in range(2):
+        rank = jnp.sum(jnp.where(named[j], before, 0.0), axis=1, keepdims=True)
+        placed = jnp.where(lane == 4 + j, placed[:, j : j + 1] * cap + rank, placed)
+    route_col[...] = placed
+    slot_row[...] = jnp.transpose(placed)[0:8, :]
+
+    dispatch(group_masks[2][0])
     for mask in group_masks[0]:
         if mask:
             dispatch(mask)
@@ -247,7 +331,6 @@
         return carry
 
     lax.fori_loop(0, block_count, gather_block, 0)
-    st_send[...] = cst[block_count].astype(BF16)
     st_buf[slot] = cst[block_count].astype(BF16)
     s_copy = {
         mask: start(
@@ -257,7 +340,8 @@
     }
     t_copy = {
         mask: start(
-            remote(st_send, st_buf.at[slot], t_send.at[mask], t_recv.at[mask], peer(mask))
+            remote(
+                st_buf.at[slot], st_buf.at[slot], t_send.at[mask], t_recv.at[mask], peer(mask))
         )
         for mask in range(1, half)
     }
@@ -266,6 +350,7 @@
     for mask in group_masks[1][: per_group // 2]:
         dispatch(mask)
 
+    keep_own()
     for mask in range(1, n):
         s_copy[mask].wait_recv()
     for mask in range(1, half):
@@ -297,8 +382,10 @@
     for mask in group_masks[1][per_group // 2 :]:
         dispatch(mask)
 
-    for mask in group_masks[2]:
+    for i, mask in enumerate(group_masks[2]):
         forward_x(mask)
+        for e in range(i, local_experts if i + 1 == per_group else min(i + 1, local_experts)):
+            send_down(3, e)
 
     logs, valid, suffix = [None] * half, [None] * half, jnp.zeros((1, LANES), F32)
     for j in reversed(range(half)):
@@ -325,7 +412,7 @@
         summed = low_in[:, h : h + 1] * low_buf[h].astype(F32)
         for j in range(half):
             summed = summed + weights[j][:, h : h + 1] * st_buf[j, h].astype(F32)
-        cin[h] = summed
+        cst[0, h] = summed
 
     loads["q"].wait()
     scale = 1.0 / math.sqrt(key_width)
@@ -347,7 +434,7 @@
             highest = jnp.maximum(carried, jnp.max(log_weight, axis=1, keepdims=True))
             inner = (scores * jnp.exp(log_weight - highest)).astype(BF16)
             memory = (
-                tabs[TWI, pl.ds(b, 1), h : h + 1] * cin[h]
+                tabs[TWI, pl.ds(b, 1), h : h + 1] * cst[0, h]
                 + tabs[TWL, pl.ds(b, 1), h : h + 1] * cst[b, h]
             ).astype(BF16)
             state = jnp.exp(carried - highest) * dot(query, memory) + dot(inner, value)
@@ -360,17 +447,16 @@
     lax.fori_loop(0, block_count, read_block, 0)
 
     loads["wo"].wait()
-    tile = 256
 
     def project(index):
         left = hid[pl.ds(pl.multiple_of(index * part_rows, part_rows), part_rows), :]
 
         def piece(i, carry):
-            at = pl.ds(pl.multiple_of(i * tile, tile), tile)
+            at = pl.ds(pl.multiple_of(i * wide, wide), wide)
             part[index, :, at] = dot(left, wo[:, at]).astype(BF16)
             return carry
 
-        lax.fori_loop(0, model // tile, piece, 0)
+        lax.fori_loop(0, model // wide, piece, 0)
 
     m_copy = []
     for i in range(2):
@@ -387,8 +473,7 @@
             )
         )
     project(t2)
-    for copy in m_copy:
-        copy.wait_recv()
+    forward_x(group_masks[3][0])
     chunk = 32
 
     def add_other(i, carry):
@@ -398,22 +483,16 @@
         ).astype(BF16)
         return carry
 
-    lax.fori_loop(0, part_rows // chunk, add_other, 0)
-
     f_copy, h_copy = {}, {}
 
     def stage_core(g, which):
         if which == 0:
             for mask in group_masks[g]:
-                if mask == 0:
-                    loads["a0"].wait()
-                elif mask < half:
+                if 0 < mask < half:
                     a_copy[mask].wait_recv()
         else:
             for mask in group_masks[g]:
-                if mask == 0:
-                    loads["b0"].wait()
-                else:
+                if mask:
                     b_copy[mask].wait_recv()
         view = rows.at[
             :, slots(group_masks[g][0], per_group), window(t if which == 0 else t2)
@@ -466,9 +545,13 @@
         h_copy[g, 2].wait_recv()
         if not down_ready:
             loads["down"].wait()
-            for mask in (1, 2, 3):
-                w_copy[mask].wait_recv()
+            for copy in w_copy.values():
+                copy.wait_recv()
             down_ready.append(True)
+        for mask in group_masks[g]:
+            if mask:
+                a_copy[mask].wait_send()
+                sent.add(id(a_copy[mask]))
 
         def one(i, carry):
             e, c = i // (width // tile), i % (width // tile)
@@ -484,57 +567,126 @@
             if mask:
                 r_copy[mask] = start(
                     remote(
-                        view, ret_ref.at[mask], r_send.at[mask], r_recv.at[mask], peer(mask)
+                        view,
+                        ret.at[:, slots(mask), :],
+                        r_send.at[mask],
+                        r_recv.at[mask],
+                        peer(mask),
                     )
                 )
             else:
-                load("ret", view, ret_ref.at[0])
+                load("ret", view, ret.at[:, slots(0), :])
+
+    x_copy = []
+    pieces = 4
+
+    def send_mixed(i):
+        at = pl.ds(i * (part_rows // pieces), part_rows // pieces)
+        x_copy.append(
+            start(
+                remote(
+                    part.at[t2, at],
+                    xrecv.at[at],
+                    m_send.at[2 + i],
+                    m_recv.at[2 + i],
+                    {"tp": t2},
+                )
+            )
+        )
 
     stage_core(2, 0)
     stage_core(2, 1)
-    x_copy = start(
-        remote(part.at[t2], xrecv, m_send.at[2], m_recv.at[2], {"tp": t2})
-    )
     stage_core(0, 0)
     stage_core(0, 1)
-    project(t)
     stage_hidden(2)
     stage_hidden(0)
+    for copy in m_copy:
+        copy.wait_recv()
+    lax.fori_loop(0, part_rows // chunk, add_other, 0)
+    send_mixed(0)
     stage_units(2)
-    for mask in group_masks[3]:
+    stage_down(2)
+    for mask in group_masks[3][1:]:
         forward_x(mask)
+    stage_units(0)
+    stage_down(0)
     stage_core(3, 0)
-    stage_units(0)
-    stage_down(2)
-    stage_core(3, 1)
     stage_core(1, 0)
     stage_core(1, 1)
-    stage_down(0)
+    stage_core(3, 1)
     stage_hidden(3)
+    send_mixed(1)
     stage_hidden(1)
+    send_mixed(2)
+    send_mixed(3)
     stage_units(3)
+    stage_down(3)
+    project(t)
     stage_units(1)
-    stage_down(3)
     stage_down(1)
-
-    x_copy.wait_recv()
-
     def add_own(i, carry):
         at = pl.ds(pl.multiple_of(i * chunk, chunk), chunk)
-        mixed_ref[at, :] = (
+        xrecv[at, :] = (
             part[t, at, :].astype(F32)
             + crecv[side, at, :].astype(F32)
             + xrecv[at, :].astype(F32)
         ).astype(BF16)
         return carry
 
+    across = width // tile
+
+    def combine(g, first, last):
+        for mask in group_masks[g]:
+            if mask:
+                r_copy[mask].wait_recv()
+            else:
+                loads["ret"].wait()
+        length = per_group * cap
+        place = lax.broadcasted_iota(jnp.int32, (BLOCK, length), 1)
+        ids = []
+        for e in range(local_experts):
+            found = jnp.zeros((BLOCK, length), jnp.int32)
+            for i, mask in enumerate(group_masks[g]):
+                begin = (flip(me, mask) * local_experts + e) * cap - i * cap
+                found = jnp.where(place >= i * cap, place + begin, found)
+            ids.append(found.astype(F32))
+
+        def row_tile(i, carry):
+            at = pl.ds(pl.multiple_of(i * BLOCK, BLOCK), BLOCK)
+            picks = []
+            for e in range(local_experts):
+                found = [
+                    jnp.where(route_col[at, 4 + j : 5 + j] == ids[e], 1.0, 0.0) for j in range(2)
+                ]
+                picks.append(jnp.concatenate(found, axis=0).astype(BF16))
+            for j in range(across):
+                cut = slice(j * tile, (j + 1) * tile)
+                both = sum(
+                    dot(picks[e], ret[e, group_slots(g), cut]) for e in range(local_experts)
+                )
+                total = route_col[at, 2:3] * both[:BLOCK] + route_col[at, 3:4] * both[BLOCK:]
+                where = i * across + j
+                held = (where // head_count, where % head_count)
+                if not first:
+                    total = total + cst[held[0], held[1]]
+                if last:
+                    routed_ref[at, cut] = total.astype(BF16)
+                else:
+                    cst[held[0], held[1]] = total
+            return carry
+
+        lax.fori_loop(0, token_count // BLOCK, row_tile, 0)
+
+    combine(0, True, False)
+    combine(2, False, False)
+    combine(1, False, False)
+    for copy in x_copy:
+        copy.wait_recv()
     lax.fori_loop(0, part_rows // chunk, add_own, 0)
-
-    loads["ret"].wait()
-    for mask in range(1, n):
-        r_copy[mask].wait_recv()
+    combine(3, False, True)
     for copy in sends:
-        copy.wait_send()
+        if id(copy) not in sent:
+            copy.wait_send()
 
     @pl.when(me < half)
     def _():
@@ -587,7 +739,6 @@
     pick_count = expert_choice_index.shape[1]
     local_experts, _, units = gate_weight.shape
     n, tp = lax.axis_size("ep"), lax.axis_size("tp")
-    me, t = lax.axis_index("ep"), lax.axis_index("tp")
     half = n // 2
     expert_count = local_experts * n
     cap = tp * max(1, 3 * pick_count * token_count // (2 * expert_count * tp))
@@ -598,39 +749,6 @@
     block_count = row_count // BLOCK
     out_depth = head_count * value_width
 
-    share = expert_raw_weight / jnp.sum(expert_raw_weight, axis=1, keepdims=True)
-    route_weight = group_likelihood[:, None] * share
-
-    experts = jnp.arange(expert_count, dtype=jnp.int32)
-    named = expert_choice_index[:, :, None] == experts
-    named_token = jnp.sum(named.astype(F32), axis=1)
-    earlier = jnp.tril(jnp.ones((token_count, token_count), BF16), -1)
-    before = jnp.dot(earlier, named_token.astype(BF16), preferred_element_type=F32)
-    slot_rank = jnp.sum(jnp.where(named, before[:, None, :], 0.0), axis=2).astype(jnp.int32)
-    slot_index = expert_choice_index * cap + slot_rank
-
-    send_shape = (n, local_experts, cap)
-    step, expert, row = (lax.broadcasted_iota(jnp.int32, send_shape, i) for i in range(3))
-    send_slot = (((me ^ step) * local_experts + expert) * cap + row).reshape(-1)
-
-    token_float = second_micro_tokens.astype(F32)
-    inverse = lax.rsqrt(jnp.mean(token_float * token_float, axis=-1, keepdims=True) + EPSILON)
-
-    def normed(index):
-        tokens = lax.dynamic_slice_in_dim(second_micro_tokens, index * width, width, 1)
-        gain = lax.dynamic_slice_in_dim(expert_norm_scale, index * width, width, 0)
-        return (tokens.astype(F32) * inverse * gain).astype(BF16)
-
-    chosen = send_slot[:, None] == slot_index[:, 0][None, :]
-    for pick in range(1, pick_count):
-        chosen = chosen | (send_slot[:, None] == slot_index[:, pick][None, :])
-    chosen = chosen.astype(BF16)
-    near = half * local_experts * cap
-    out_a = jnp.dot(chosen, normed(t), preferred_element_type=F32).astype(BF16)
-    out_b = jnp.dot(chosen[:near], normed(t ^ 2), preferred_element_type=F32).astype(BF16)
-    out_a = out_a.reshape(n, local_experts, cap, width)
-    out_b = out_b.reshape(half, local_experts, cap, width)
-
     cols, arow, gp = gates(log_input_gate, forget_preactivation, forget_offset, key_width)
 
     slot_rows = n * cap
@@ -638,14 +756,14 @@
     vmem = pl.BlockSpec(memory_space=pltpu.VMEM)
     hbm = pl.BlockSpec(memory_space=pl.ANY)
     dma = pltpu.SemaphoreType.DMA
-    mixed, returned = pl.pallas_call(
-        functools.partial(kernel, n, tp),
+    mixed, routed = pl.pallas_call(
+        functools.partial(kernel, n, tp, cap),
         out_shape=(
             jax.ShapeDtypeStruct((part_rows, model_width), BF16),
-            jax.ShapeDtypeStruct((n, local_experts, cap, width), BF16),
+            jax.ShapeDtypeStruct((token_count, width), BF16),
         ),
-        in_specs=[hbm] * 5 + [vmem] * 4 + [hbm] * 4,
-        out_specs=(vmem, hbm),
+        in_specs=[hbm] + [vmem] * 4 + [hbm] * 3 + [vmem] * 4 + [hbm] * 4,
+        out_specs=(vmem, vmem),
         scratch_shapes=[
             pltpu.VMEM((local_experts, slot_rows, model_width), BF16),
             pltpu.VMEM(gate_weight.shape, BF16),
@@ -655,22 +773,24 @@
             pltpu.VMEM((local_experts, slot_rows, width), BF16),
             pltpu.VMEM((tp, part_rows, model_width), BF16),
             pltpu.VMEM((2, part_rows, model_width), BF16),
-            pltpu.VMEM((part_rows, model_width), BF16),
             pltpu.VMEM(queries.shape, BF16),
             pltpu.VMEM(keys.shape, BF16),
             pltpu.VMEM(values.shape, BF16),
             pltpu.VMEM((row_count, out_depth), BF16),
             pltpu.VMEM((out_depth, model_width), BF16),
             pltpu.VMEM((block_count + 1, head_count, key_width, value_width), F32),
-            pltpu.VMEM((head_count, key_width, value_width), F32),
             pltpu.VMEM((7, block_count, LANES), F32),
             pltpu.VMEM((8, LANES), F32),
             pltpu.VMEM((n, 8, LANES), F32),
-            pltpu.VMEM((head_count, key_width, value_width), BF16),
             pltpu.VMEM((half, head_count, key_width, value_width), BF16),
             pltpu.VMEM((head_count, key_width, value_width), BF16),
             pltpu.VMEM((head_count, key_width, value_width), BF16),
-            dma((10,)),
+            pltpu.VMEM((local_experts, slot_rows, width), BF16),
+            pltpu.VMEM((token_count, width), BF16),
+            pltpu.VMEM((half - 1, local_experts, cap, width), BF16),
+            pltpu.VMEM((token_count, LANES), F32),
+            pltpu.VMEM((8, token_count), F32),
+            dma((12,)),
             dma((n,)),
             dma((n,)),
             dma((n,)),
@@ -679,16 +799,16 @@
             dma((2, 4)),
             dma((3, 4)),
             dma((3, 4)),
-            dma((tp,)),
-            dma((tp,)),
+            dma((tp, local_experts)),
+            dma((tp, local_experts)),
             dma((n,)),
             dma((n,)),
             dma((half,)),
             dma((half,)),
             dma((1,)),
             dma((1,)),
-            dma((3,)),
-            dma((3,)),
+            dma((6,)),
+            dma((6,)),
             dma((n,)),
             dma((n,)),
         ],
@@ -697,8 +817,11 @@
         ),
         name="exchange",
     )(
-        out_a,
-        out_b,
+        second_micro_tokens.reshape(-1, part_rows, model_width),
+        expert_norm_scale.reshape(1, -1),
+        expert_choice_index.T,
+        group_likelihood.reshape(1, -1),
+        expert_raw_weight.T,
         queries,
         keys,
         values,
@@ -711,21 +834,7 @@
         up_weight,
         down_weight,
     )
-    returned = returned.reshape(-1, width)
-
-    spread = jnp.zeros((token_count, send_slot.shape[0]), F32)
-    for pick in range(pick_count):
-        spread = spread + jnp.where(
-            slot_index[:, pick : pick + 1] == send_slot[None, :],
-            route_weight[:, pick : pick + 1],
-            0.0,
-        )
-    spread_high = spread.astype(BF16)
-    spread_low = (spread - spread_high.astype(F32)).astype(BF16)
-    combined = jnp.dot(spread_high, returned, preferred_element_type=F32) + jnp.dot(
-        spread_low, returned, preferred_element_type=F32
-    )
-    return mixed, combined.astype(BF16)
+    return mixed, routed
 
 
 def solution(mesh):

time: 231 us -> 190 us (0.82)
  Pallas kernels: 201 us -> 180 us
  matrix products: 13.6 us -> 0.17 us
  other arithmetic: 8.56 us -> 2.91 us
    pallas_call x1, Pallas kernels: 201 us -> 180 us  [per_device(): pl.pallas_call(functools.partial(kernel, n, tp, cap), out_shape=(jax.Shap...]
    dot_general x5 -> x0, matrix products: 13.4 us -> none  [the longest x1 4.04 us: per_device(): jnp.dot(spread_low, returned, preferred_element_type=F32)]
    reduce_sum x4 -> x0, other arithmetic: 5.36 us -> none  [the longest x1 3.24 us: per_device(): jnp.mean(token_float * token_float, axis=-1, keepdims=True) + EPSILON]
    unnamed x25 -> x4, local copies, waits for them, and re-layouts: 1.58 us -> 4.19 us
where the time goes in v1:
time: 190 us; the launch traced here: 189 us
  Pallas kernels  180 us (95%)
  local copies, waits for them, and re-layouts  6.11 us (3%)
  other arithmetic  2.91 us (2%)
    pallas_call x1, Pallas kernels, per_device(): pl.pallas_call(functools.partial(kernel, n, tp, cap), out_shape=(jax.Shap...  180 us
    unnamed x4, local copies, waits for them, and re-layouts  4.19 us

profile of v1, /device:TPU:0, one launch (start us, length us, event | category | flops | bytes accessed | tf_op | source)
XLA Modules:
  0.0 189.4 jit_solution(4010961443642783038)
XLA Ops:
  0.6 0.7 fusion.6
  1.4 0.2 convolution_bitcast_fusion
  1.5 0.2 slice_reduce_fusion
  1.7 0.9 fusion.10
  2.6 0.1 copy.25
  2.7 0.6 pad.4.gp_ref
  3.3 1.3 fusion.7
  4.6 1.0 copy.24
  5.6 179.5 %exchange.1 = (bf16[256,4096]{1,0:T(8,128)(2,1)}, bf16[512,1024]{1,0:T(8,128)(2,1)}) custom-call(bf16[2,256,4096]{2,1,0:T(8,128)(2,1)} %bitcast.37, f32[1,4096]{1,0:T(1,128)} %bitcast.41, s32[2,512]{1,0:T(2,128)} %bitcast.44, f32[1,512]{1,0:T(1,128)} %bitcast.46, f32[2,512]{1,0:T(2,128)} %bitcast.45, bf16[1024,256]{1,0:T(8,128)(2,1)} %q_hbm.1, ...), custom_call_target="tpu_custom_call" | custom-call | tf_op jit(solution)/shard_map/exchange/pallas_call | solution.py:759
  185.2 0.0 copy-start
  185.2 3.2 %copy.40 = bf16[256,4096]{1,0:T(8,128)(2,1)} copy(bf16[256,4096]{1,0:T(8,128)(2,1)} %get-tuple-element.6) | data formatting | bytes 4194304
  188.4 0.0 copy-done
  188.4 1.0 copy.41
  (2 shorter events, 0.0 us)
Async XLA Ops:
  185.2 3.2 %copy-start = (bf16[512,1024]{1,0:T(8,128)(2,1)S(1)}, bf16[512,1024]{1,0:T(8,128)(2,1)}, u32[]{:S(2)}) copy-start(bf16[512,1024]{1,0:T(8,128)(2,1)} %get-tuple-element.7) | copy-start | bytes 3145732

commit v2 on v1

--- a/solution.py
+++ b/solution.py
@@ -42,9 +42,9 @@
     q_hbm,
     k_hbm,
     v_hbm,
-    cols_ref,
-    arow_ref,
-    gp_ref,
+    in_gate_ref,
+    forget_ref,
+    offset_ref,
     hscale_ref,
     wo_hbm,
     gate_hbm,
@@ -77,6 +77,8 @@
     bbuf,
     route_col,
     slot_row,
+    arow_ref,
+    cols_ref,
     load_sem,
     a_send,
     a_recv,
@@ -296,10 +298,48 @@
             dispatch(mask)
 
     TQ, TC, TW1, TW2, TF, TWI, TWL = range(7)
+    pair_count = block_count * head_count
+    scale = 1.0 / math.sqrt(key_width)
+    high = lax.Precision.HIGHEST
+
+    def exact(left, right):
+        return lax.dot_general(
+            left, right, (((1,), (0,)), ((), ())), precision=high, preferred_element_type=F32
+        )
+
+    row_at = lax.broadcasted_iota(jnp.int32, (BLOCK, BLOCK), 0)
+    lane_at = lax.broadcasted_iota(jnp.int32, (BLOCK, BLOCK), 1)
+    forget = forget_ref[...]
+    forget_log = jnp.minimum(forget, 0.0) - jnp.log1p(jnp.exp(-jnp.abs(forget)))
+    forget_log = forget_log + offset_ref[...]
+    running_rows = exact(forget_log, jnp.where(row_at <= lane_at, 1.0, 0.0))
+    spans = running_rows[:, BLOCK - 1 : BLOCK]
+    to_end = spans - running_rows + in_gate_ref[...]
+    peaks = jnp.max(to_end, axis=1, keepdims=True)
+    key_rows = jnp.exp(to_end - peaks) * scale
+    arow_ref[...] = in_gate_ref[...] - running_rows
+    tall = jnp.concatenate(
+        [running_rows, key_rows, jnp.zeros((BLOCK - 2 * pair_count, BLOCK), F32)], axis=0
+    )
+    cols_ref[...] = jnp.transpose(tall)
+    pair_row = lax.broadcasted_iota(jnp.int32, (pair_count, LANES), 0)
+    pair_lane = lax.broadcasted_iota(jnp.int32, (pair_count, LANES), 1)
+    of_head = pair_lane == pair_row % head_count
+    block_row = lax.broadcasted_iota(jnp.int32, (block_count, pair_count), 0)
+    block_lane = lax.broadcasted_iota(jnp.int32, (block_count, pair_count), 1)
+    of_block = jnp.where(block_lane // head_count == block_row, 1.0, 0.0)
+    span_table = exact(of_block, jnp.where(of_head, spans, 0.0))
+    peak_table = exact(of_block, jnp.where(of_head, peaks, 0.0))
+
+    def column(index):
+        return jnp.sum(
+            jnp.where(lane_at == index, cols_ref[...], 0.0), axis=1, keepdims=True
+        )
+
     stable = jnp.full((1, LANES), FLOOR_LOG, F32)
     total = jnp.zeros((1, LANES), F32)
     for b in range(block_count):
-        span, peak = gp_ref[0, b : b + 1, :], gp_ref[1, b : b + 1, :]
+        span, peak = span_table[b : b + 1, :], peak_table[b : b + 1, :]
         tabs[TQ, b : b + 1, :] = total
         tabs[TC, b : b + 1, :] = stable
         newer = jnp.maximum(span + stable, peak)
@@ -319,7 +359,7 @@
         at = pl.ds(pl.multiple_of(b * BLOCK, BLOCK), BLOCK)
         for h in range(head_count):
             keyed = kb[at, h * key_width : (h + 1) * key_width].astype(F32)
-            weight = cols_ref[at, head_count + h : head_count + h + 1]
+            weight = column(pair_count + b * head_count + h)
             update = dot(
                 (keyed * weight).astype(BF16),
                 vb[at, h * value_width : (h + 1) * value_width],
@@ -415,10 +455,7 @@
         cst[0, h] = summed
 
     loads["q"].wait()
-    scale = 1.0 / math.sqrt(key_width)
-    causal = lax.broadcasted_iota(jnp.int32, (BLOCK, BLOCK), 0) >= lax.broadcasted_iota(
-        jnp.int32, (BLOCK, BLOCK), 1
-    )
+    causal = row_at >= lane_at
 
     def read_block(b, carry):
         at = pl.ds(pl.multiple_of(b * BLOCK, BLOCK), BLOCK)
@@ -426,8 +463,8 @@
             query = qb[at, h * key_width : (h + 1) * key_width]
             key = kb[at, h * key_width : (h + 1) * key_width]
             value = vb[at, h * value_width : (h + 1) * value_width]
-            running = cols_ref[at, h : h + 1]
-            other = arow_ref[pl.ds(h * block_count + b, 1), :]
+            running = column(b * head_count + h)
+            other = arow_ref[pl.ds(b * head_count + h, 1), :]
             scores = dot(query, key, ((1,), (1,))) * scale
             log_weight = jnp.where(causal, running + other, FLOOR_LOG)
             carried = running + tabs[TF, pl.ds(b, 1), h : h + 1]
@@ -603,11 +640,11 @@
     for copy in m_copy:
         copy.wait_recv()
     lax.fori_loop(0, part_rows // chunk, add_other, 0)
-    send_mixed(0)
     stage_units(2)
     stage_down(2)
     for mask in group_masks[3][1:]:
         forward_x(mask)
+    send_mixed(0)
     stage_units(0)
     stage_down(0)
     stage_core(3, 0)
@@ -693,28 +730,10 @@
         l_copy.wait_send()
 
 
-def gates(log_input_gate, forget_preactivation, forget_offset, key_width):
-    row_count, head_count = log_input_gate.shape
-    block_count = row_count // BLOCK
-    forget_log = jax.nn.log_sigmoid(forget_preactivation) + forget_offset
-    forget_log = forget_log.reshape(block_count, BLOCK, head_count)
-    in_gate = log_input_gate.reshape(block_count, BLOCK, head_count)
-    lower = jnp.tril(jnp.ones((BLOCK, BLOCK), F32))
-    running = jnp.einsum(
-        "ts,bsh->bth",
-        lower,
-        forget_log,
-        preferred_element_type=F32,
-        precision=lax.Precision.HIGHEST,
-    )
-    totals = running[:, -1]
-    to_end = totals[:, None] - running + in_gate
-    peak = jnp.max(to_end, axis=1)
-    key_weight = jnp.exp(to_end - peak[:, None]) * (1.0 / math.sqrt(key_width))
-    cols = jnp.concatenate([running, key_weight], axis=2).reshape(row_count, -1)
-    arow = (in_gate - running).transpose(2, 0, 1).reshape(head_count * block_count, BLOCK)
-    gp = jnp.pad(jnp.stack([totals, peak]), ((0, 0), (0, 0), (0, LANES - head_count)))
-    return cols, arow, gp
+def by_block(gate):
+    row_count, head_count = gate.shape
+    gate = gate.reshape(row_count // BLOCK, BLOCK, head_count).transpose(0, 2, 1)
+    return gate.reshape(-1, BLOCK)
 
 
 def per_device(
@@ -748,8 +767,6 @@
     value_width = values.shape[1] // head_count
     block_count = row_count // BLOCK
     out_depth = head_count * value_width
-
-    cols, arow, gp = gates(log_input_gate, forget_preactivation, forget_offset, key_width)
 
     slot_rows = n * cap
     part_rows = row_count // tp
@@ -790,6 +807,8 @@
             pltpu.VMEM((half - 1, local_experts, cap, width), BF16),
             pltpu.VMEM((token_count, LANES), F32),
             pltpu.VMEM((8, token_count), F32),
+            pltpu.VMEM((block_count * head_count, BLOCK), F32),
+            pltpu.VMEM((BLOCK, BLOCK), F32),
             dma((12,)),
             dma((n,)),
             dma((n,)),
@@ -825,9 +844,9 @@
         queries,
         keys,
         values,
-        cols,
-        arow,
-        gp,
+        by_block(log_input_gate),
+        by_block(forget_preactivation),
+        by_block(forget_offset),
         head_norm_scale.reshape(1, -1),
         memory_output_weight,
         gate_weight,

time: 190 us -> 183 us (0.963)
  other arithmetic: 2.91 us -> 0 us
  Pallas kernels: 180 us -> 178 us
  local copies, waits for them, and re-layouts: 6.11 us -> 4.19 us
where the time goes in v2:
time: 183 us
  Pallas kernels  178 us (97%)
  local copies, waits for them, and re-layouts  4.19 us (2%)
    pallas_call x1, Pallas kernels, per_device(): pl.pallas_call(functools.partial(kernel, n, tp, cap), out_shape=(jax.Shap...  178 us
    unnamed x4, local copies, waits for them, and re-layouts  4.19 us

profile of v2, /device:TPU:0, one launch (start us, length us, event | category | flops | bytes accessed | tf_op | source)
XLA Modules:
  0.0 182.8 jit_solution(4240373460159041795)
XLA Ops:
  0.6 177.9 %exchange.1 = (bf16[256,4096]{1,0:T(8,128)(2,1)}, bf16[512,1024]{1,0:T(8,128)(2,1)}) custom-call(bf16[2,256,4096]{2,1,0:T(8,128)(2,1)} %bitcast.21, f32[1,4096]{1,0:T(1,128)} %bitcast.22, s32[2,512]{1,0:T(2,128)} %bitcast.26, f32[1,512]{1,0:T(1,128)} %bitcast.28, f32[2,512]{1,0:T(2,128)} %bitcast.27, bf16[1024,256]{1,0:T(8,128)(2,1)} %q_hbm.1, ...), custom_call_target="tpu_custom_call" | custom-call | tf_op jit(solution)/shard_map/exchange/pallas_call | solution.py:776
  178.6 0.0 copy-start
  178.6 3.2 %copy.23 = bf16[256,4096]{1,0:T(8,128)(2,1)} copy(bf16[256,4096]{1,0:T(8,128)(2,1)} %get-tuple-element.4) | data formatting | bytes 4194304
  181.8 0.0 copy-done
  181.8 1.0 copy.24
Async XLA Ops:
  178.6 3.2 %copy-start = (bf16[512,1024]{1,0:T(8,128)(2,1)S(1)}, bf16[512,1024]{1,0:T(8,128)(2,1)}, u32[]{:S(2)}) copy-start(bf16[512,1024]{1,0:T(8,128)(2,1)} %get-tuple-element.5) | copy-start | bytes 3145732
